TPU v7x, 32 devices: a whole 2x2x4 slice. The times are simulated.
32 devices in a mesh: sp: 8 (over z, core), tp: 4 (over y, x).
Axes of the slice: x: 2, y: 2, z: 4, core: 2. Of those that a mesh axis runs over, the one named last changes fastest.
Arguments:
- prompt: bfloat16 [8, 2048, 2048], P('tp', 'sp'), may hold values from -6 to 6
- input_gain: float32 [2048], replicated, may hold values from 0.1 to 1.9
- key_weight: bfloat16 [1024, 2048], P('tp'), may hold values from -0.125 to 0.125
- value_weight: bfloat16 [1024, 2048], P('tp'), may hold values from -0.125 to 0.125
- key_gain: float32 [64], replicated, may hold values from 0.1 to 1.9
- queries: bfloat16 [8, 2, 1024], P('sp', None, 'tp'), may hold values from -6 to 6
- score_bias: float32 [2, 16], replicated, may hold values from -9 to -2
Outputs:
- keys: bfloat16 [8, 1024, 2048], P('sp', 'tp')
- values: bfloat16 [8, 1024, 2048], P('sp', 'tp')
- first_read: bfloat16 [8, 2, 1024], P('sp', None, 'tp')
All inputs are finite; a program needn't handle non-finite values.
Results may differ from a plain program's by a relative error of at most 0.01.
Values may be sent and summed in bfloat16 or wider, within the bound.
No kernel may reach another device: no remote copies, remote signals or barrier semaphores. Data moves between devices by JAX's collectives and lax.ppermute only.
A program may use at most 64 MiB of HBM per device.

v0:
```python
import math
import jax
import jax.numpy as jnp
from jax import lax
from jax.sharding import PartitionSpec as P

HEAD = 64
epsilon = 1e-06


def local(prompt, input_gain, key_weight, value_weight, key_gain, queries, score_bias):
    seq_here, pos_here, width = prompt.shape
    flat = prompt.astype(jnp.float32)
    normed = (
        flat * lax.rsqrt(jnp.mean(flat * flat, axis=-1, keepdims=True) + epsilon) * input_gain
    ).astype(jnp.bfloat16)
    stacked = jnp.stack([key_weight, value_weight])
    columns = key_weight.shape[0]
    kv_width = columns * lax.axis_size("tp")
    projected = jnp.einsum(
        "spd,knd->sknp",
        normed,
        lax.all_gather(stacked, "tp", axis=1, tiled=True),
        preferred_element_type=jnp.float32,
    )
    key_raw = projected[:, 0].reshape(seq_here, kv_width // HEAD, HEAD, pos_here)
    key_norm = (
        key_raw
        * lax.rsqrt(jnp.mean(key_raw * key_raw, axis=2, keepdims=True) + epsilon)
        * key_gain[:, None]
    )
    key_rows = key_norm.reshape(seq_here, kv_width, pos_here).astype(jnp.bfloat16)
    value_rows = projected[:, 1].astype(jnp.bfloat16)
    packed = jnp.stack([key_rows, value_rows], axis=1)
    by_sequence = lax.all_to_all(
        lax.all_to_all(packed, "tp", split_axis=2, concat_axis=0, tiled=True),
        "sp",
        split_axis=0,
        concat_axis=3,
        tiled=True,
    )
    keys = by_sequence[:, 0]
    values = by_sequence[:, 1]
    length = keys.shape[2]
    group = queries.shape[1]
    heads_here = columns // HEAD
    query_heads = queries[0].reshape(group, heads_here, HEAD)
    cache_keys = keys[0].reshape(heads_here, HEAD, length)
    scores = jnp.einsum("ghd,hds->ghs", query_heads, cache_keys, preferred_element_type=jnp.float32)
    first_head = lax.axis_index("tp") * heads_here
    offsets = lax.dynamic_slice_in_dim(score_bias, first_head, heads_here, 1)
    scores = scores / math.sqrt(HEAD) + offsets[:, :, None]
    log_break = jax.nn.log_sigmoid(scores)
    log_keep = jax.nn.log_sigmoid(-scores)
    later = lax.cumsum(log_keep, axis=2, reverse=True) - log_keep
    weights = jnp.exp(log_break + later).astype(jnp.bfloat16)
    cache_values = values[0].reshape(heads_here, HEAD, length)
    first_read = jnp.einsum(
        "ghs,hds->ghd", weights, cache_values, preferred_element_type=jnp.float32
    )
    first_read = first_read.astype(jnp.bfloat16).reshape(1, group, columns)
    return (keys, values, first_read)


def solution(mesh):
    placed = (P("tp", "sp", None), P(), P("tp", None), P("tp", None), P(), P("sp", None, "tp"), P())
    return jax.shard_map(
        local,
        mesh=mesh,
        in_specs=placed,
        out_specs=(P("sp", "tp", None), P("sp", "tp", None), P("sp", None, "tp")),
        check_vma=False,
    )
```

profile of v0, /device:TPU:0, one launch (start us, length us, event | category | flops | bytes accessed | tf_op | source)
XLA Modules:
  0.0 230.0 jit_solution(6662935200432588919)
XLA Ops:
  7.2 3.1 %pad_maximum_fusion = bf16[2,256,2048]{2,1,0:T(8,128)(2,1)} fusion(bf16[1,256,2048]{2,1,0:T(8,128)(2,1)} %bitcast.54, bf16[1,256,2048]{2,1,0:T(8,128)(2,1)} %bitcast.55), kind=kLoop, calls=%fused_computation.13 | loop fusion | flops 1048576 | bytes 4194304 | tf_op jit(solution)/shard_map/stack | solution.py:17
  10.4 0.6 copy-done.7
  11.1 0.9 copy-done.5
  11.9 0.5 fusion.2
  12.4 88.3 %all-gather.2.cloned.1.call-done = bf16[2,1024,2048]{2,1,0:T(8,128)(2,1)} async-done(((bf16[2,256,2048]{2,1,0:T(8,128)(2,1)}), bf16[2,1024,2048]{2,1,0:T(8,128)(2,1)}) %all-gather.2.cloned.1.call-update) | async-done | bytes 8388624 | tf_op jit(solution)/shard_map/all_gather | solution.py:23
  100.7 7.1 %fusion.7 = f32[2,2,1024,256]{3,2,0,1:T(8,128)S(1)} fusion(bf16[2,1024,2048]{2,1,0:T(8,128)(2,1)} %all-gather.2.cloned.1.call-done, bf16[2,256,2048]{2,1,0:T(8,128)(2,1)S(1)} %copy-done.5, f32[2048]{0:T(1024)S(1)} %copy-done.8, f32[2,256]{1,0:T(2,128)S(1)} %add_rsqrt_fusion.1), kind=kOutput, calls=%fused_computation.10 | convolution fusion | flops 4299161600 | bytes 14690304 | tf_op jit(solution)/shard_map/spd,knd->sknp/dot_general | solution.py:20
  108.0 1.8 copy-done.2
  110.2 1.9 fusion.13
  112.2 2.2 copy.42
  114.4 28.0 %all_to_all.36 = bf16[2,2,1024,256]{3,0,1,2:T(2,128)(2,1)S(1)} all-to-all(bf16[2,2,1024,256]{3,0,1,2:T(2,128)(2,1)S(1)} %copy.42), channel_id=1, replica_groups=mesh['sp'=8,'tp'=4] {'tp'}, dimensions={2} | all-to-all | bytes 4194304 | tf_op jit(solution)/shard_map/all_to_all | solution.py:36
  142.6 1.5 copy.44
  144.1 4.7 %all-to-all-start.1 = ((bf16[8,2,256,256]{3,2,1,0:T(8,128)(2,1)}), bf16[8,2,256,256]{3,2,1,0:T(8,128)(2,1)S(1)}, u32[]{:S(2)}, u32[]{:S(2)}) async-start(bf16[8,2,256,256]{3,2,1,0:T(8,128)(2,1)} %bitcast.49), calls=%async_computation.1 | async-start | bytes 4194304 | tf_op jit(solution)/shard_map/all_to_all | solution.py:35
  149.1 48.8 %all-to-all-done.1 = bf16[8,2,256,256]{3,2,1,0:T(8,128)(2,1)S(1)} async-done(((bf16[8,2,256,256]{3,2,1,0:T(8,128)(2,1)}), bf16[8,2,256,256]{3,2,1,0:T(8,128)(2,1)S(1)}, u32[]{:S(2)}, u32[]{:S(2)}) %all-to-all-start.1) | async-done | bytes 2097184 | tf_op jit(solution)/shard_map/all_to_all | solution.py:35
  197.9 1.3 copy-done.1
  199.2 2.8 %copy.45 = bf16[1,2,256,8,256]{2,4,3,1,0:T(8,128)(2,1)S(1)} copy(bf16[1,2,256,8,256]{4,2,1,3,0:T(8,128)(2,1)} %bitcast.48) | data formatting | bytes 4194304 | tf_op jit(solution)/shard_map/all_to_all | solution.py:35
  202.1 1.8 fusion.27
  203.9 1.6 copy.47
  205.8 9.9 %reduce-window.6 = f32[2,4,16,128]{3,2,1,0:T(8,128)S(1)} reduce-window(f32[2,4,16,128]{3,2,1,0:T(8,128)S(1)} %copy.50, f32[]{:T(128)} %constant.9.clone.1), window={size=1x1x1x128 pad=0_0x0_0x0_0x0_127}, to_apply=%region_2.3 | reduce-window | flops 2080768 | bytes 131076 | tf_op jit(solution)/shard_map/reduce-window
  215.9 0.4 reduce-window.9
  216.5 1.4 copy.46
  217.9 1.7 fusion.16
  219.7 0.6 reshape.46
  220.3 1.4 copy.53
  221.7 1.4 copy.54
  (36 shorter events, 2.0 us)
Async XLA Ops:
  7.2 141.7 %copy-start = (f32[2,16]{1,0:T(2,128)S(1)}, f32[2,16]{1,0:T(2,128)}, u32[]{:S(2)}) copy-start(f32[2,16]{1,0:T(2,128)} %param.13) | copy-start | bytes 388
  7.2 93.5 %all-gather.2.cloned.1.call-start = ((), (), s32[]{:S(2)}) async-start(), calls=%async_computation.2 | async-start | bytes 10485760 | tf_op jit(solution)/shard_map/all_gather | solution.py:23
  10.3 0.7 copy-start.7
  10.3 1.6 copy-start.5
  10.3 90.4 %copy-start.8 = (f32[2048]{0:T(1024)S(1)}, f32[2048]{0:T(1024)}, u32[]{:S(2)}) copy-start(f32[2048]{0:T(1024)} %param.8) | copy-start | bytes 24580
  107.9 1.9 copy-start.2
  144.1 4.9 %copy-start.6 = (bf16[1,2,256]{2,1,0:T(2,128)(2,1)S(1)}, bf16[1,2,256]{2,1,0:T(2,128)(2,1)}, u32[]{:S(2)}) copy-start(bf16[1,2,256]{2,1,0:T(2,128)(2,1)} %param.12) | copy-start | bytes 3076
  144.1 53.8 %all-to-all-start.1 = ((bf16[8,2,256,256]{3,2,1,0:T(8,128)(2,1)}), bf16[8,2,256,256]{3,2,1,0:T(8,128)(2,1)S(1)}, u32[]{:S(2)}, u32[]{:S(2)}) async-start(bf16[8,2,256,256]{3,2,1,0:T(8,128)(2,1)} %bitcast.49), calls=%async_computation.1 | async-start | bytes 4194304 | tf_op jit(solution)/shard_map/all_to_all | solution.py:35
  197.9 1.3 copy-start.1
  203.9 12.6 %copy-start.4 = (bf16[1,1,256,2048]{2,3,1,0:T(8,128)(2,1)S(1)}, bf16[1,1,256,2048]{2,3,1,0:T(8,128)(2,1)}, u32[]{:S(2)}) copy-start(bf16[1,1,256,2048]{2,3,1,0:T(8,128)(2,1)} %get-tuple-element.15) | copy-start | bytes 3145732
  216.5 3.8 %copy-start.3 = (bf16[1,256,2048]{1,2,0:T(8,128)(2,1)S(1)}, bf16[1,256,2048]{1,2,0:T(8,128)(2,1)}, u32[]{:S(2)}) copy-start(bf16[1,256,2048]{1,2,0:T(8,128)(2,1)} %get-tuple-element.13) | copy-start | bytes 3145732
Sparse Core Ops, SparseCore 0:
  10.5 90.1 all-gather.1
where the time goes:
time: 230 us
  waiting for transfers between devices  137 us (60%)
  blocking collectives  28 us (12%)
  local copies, waits for them, and re-layouts  20.4 us (9%)
  other arithmetic  16.4 us (7%)
  between operations  14.2 us (6%)
  matrix products  9.17 us (4%)
  starting transfers between devices  4.77 us (2%)
    all_gather x1, waiting for transfers between devices, local(): lax.all_gather(stacked, 'tp', axis=1, tiled=True)  88.3 us
    all_to_all x1, waiting for transfers between devices, local(): lax.all_to_all(lax.all_to_all(packed, 'tp', split_axis=2, concat_axis=0,...  48.8 us
    all_to_all x1, blocking collectives, local(): lax.all_to_all(packed, 'tp', split_axis=2, concat_axis=0, tiled=True)  28 us
    another operation x2, other arithmetic  10.3 us
    unnamed x20, local copies, waits for them, and re-layouts  7.48 us
    dot_general x1, matrix products, local(): jnp.einsum('spd,knd->sknp', normed, lax.all_gather(stacked, 'tp', axis=1,...  7.13 us
    all_to_all x1, starting transfers between devices, local(): lax.all_to_all(lax.all_to_all(packed, 'tp', split_axis=2, concat_axis=0,...  4.73 us
  transfers between devices with their start and end apart: 2, of which 2 were waited for; matrix products, arithmetic and copies ran while one was open for 0% of the time, Pallas kernels for 0%

commit v1 on v0

--- a/solution.py
+++ b/solution.py
@@ -32,12 +32,17 @@
     key_rows = key_norm.reshape(seq_here, kv_width, pos_here).astype(jnp.bfloat16)
     value_rows = projected[:, 1].astype(jnp.bfloat16)
     packed = jnp.stack([key_rows, value_rows], axis=1)
+
+    def return_all_the_object(payload, dimension_no, at_axis):
+        return jnp.concatenate(
+            lax.all_to_all(
+                jnp.stack(jnp.split(payload, lax.psum(1, "tp"), dimension_no), 0), "tp", 0, 0
+            ),
+            at_axis,
+        )
+
     by_sequence = lax.all_to_all(
-        lax.all_to_all(packed, "tp", split_axis=2, concat_axis=0, tiled=True),
-        "sp",
-        split_axis=0,
-        concat_axis=3,
-        tiled=True,
+        return_all_the_object(packed, 2, 0), "sp", split_axis=0, concat_axis=3, tiled=True
     )
     keys = by_sequence[:, 0]
     values = by_sequence[:, 1]

time: 230 us -> 228 us (level)
  local copies, waits for them, and re-layouts: 20.4 us -> 17.9 us
    all_to_all x3 -> x2, local copies, waits for them, and re-layouts: 4.61 us -> 4.33 us  [the longest x1 2.85 us: local(): lax.all_to_all(return_all_the_object(packed, 2, 0), 'sp', split_axis=0, c...]
    another operation x3 -> x4, other arithmetic: 10.5 us -> 10.8 us
where the time goes in v1:
time: 228 us
  waiting for transfers between devices  137 us (60%)
  blocking collectives  28 us (12%)
  local copies, waits for them, and re-layouts  17.9 us (8%)
  other arithmetic  16.7 us (7%)
  between operations  14.2 us (6%)
  matrix products  9.17 us (4%)
  starting transfers between devices  4.77 us (2%)
    all_gather x1, waiting for transfers between devices, local(): lax.all_gather(stacked, 'tp', axis=1, tiled=True)  88.3 us
    all_to_all x1, waiting for transfers between devices, local(): lax.all_to_all(return_all_the_object(packed, 2, 0), 'sp', split_axis=0, c...  48.8 us
    all_to_all x1, blocking collectives, return_all_the_object(): lax.all_to_all(jnp.stack(jnp.split(payload, lax.psum(1, 'tp'), dimension_...  28 us
    another operation x2, other arithmetic  10.3 us
    unnamed x20, local copies, waits for them, and re-layouts  7.48 us
    dot_general x1, matrix products, local(): jnp.einsum('spd,knd->sknp', normed, lax.all_gather(stacked, 'tp', axis=1,...  7.12 us
    all_to_all x1, starting transfers between devices, local(): lax.all_to_all(return_all_the_object(packed, 2, 0), 'sp', split_axis=0, c...  4.74 us
  transfers between devices with their start and end apart: 2, of which 2 were waited for; matrix products, arithmetic and copies ran while one was open for 0% of the time, Pallas kernels for 0%

profile of v1, /device:TPU:0, one launch (start us, length us, event | category | flops | bytes accessed | tf_op | source)
XLA Modules:
  0.0 227.8 jit_solution(5218365780117662683)
XLA Ops:
  7.2 3.1 %pad_maximum_fusion = bf16[2,256,2048]{2,1,0:T(8,128)(2,1)} fusion(bf16[1,256,2048]{2,1,0:T(8,128)(2,1)} %bitcast.58, bf16[1,256,2048]{2,1,0:T(8,128)(2,1)} %bitcast.59), kind=kLoop, calls=%fused_computation.19 | loop fusion | flops 1048576 | bytes 4194304 | tf_op jit(solution)/shard_map/stack | solution.py:17
  10.4 0.6 copy-done.7
  11.1 0.9 copy-done.5
  11.9 0.5 fusion.2
  12.4 88.3 %all-gather.2.cloned.1.call-done = bf16[2,1024,2048]{2,1,0:T(8,128)(2,1)} async-done(((bf16[2,256,2048]{2,1,0:T(8,128)(2,1)}), bf16[2,1024,2048]{2,1,0:T(8,128)(2,1)}) %all-gather.2.cloned.1.call-update) | async-done | bytes 8388624 | tf_op jit(solution)/shard_map/all_gather | solution.py:23
  100.7 7.1 %fusion.7 = f32[2,2,1024,256]{3,2,0,1:T(8,128)S(1)} fusion(bf16[2,1024,2048]{2,1,0:T(8,128)(2,1)} %all-gather.2.cloned.1.call-done, bf16[2,256,2048]{2,1,0:T(8,128)(2,1)S(1)} %copy-done.5, f32[2048]{0:T(1024)S(1)} %copy-done.8, f32[2,256]{1,0:T(2,128)S(1)} %add_rsqrt_fusion.1), kind=kOutput, calls=%fused_computation.16 | convolution fusion | flops 4299161600 | bytes 14690304 | tf_op jit(solution)/shard_map/spd,knd->sknp/dot_general | solution.py:20
  108.0 1.8 copy-done.2
  110.1 1.9 fusion.13
  112.4 28.0 %all_to_all.23 = bf16[4,2,2,256,256]{4,3,1,2,0:T(8,128)(2,1)S(1)} all-to-all(bf16[4,2,2,256,256]{4,3,1,2,0:T(8,128)(2,1)S(1)} %pad_maximum_fusion.1), channel_id=1, replica_groups=mesh['sp'=8,'tp'=4] {'tp'}, dimensions={0} | all-to-all | bytes 4194304 | tf_op jit(solution)/shard_map/all_to_all | solution.py:38
  140.4 1.5 copy.20
  141.9 4.7 %all-to-all-start.1 = ((bf16[8,2,256,256]{3,2,1,0:T(8,128)(2,1)}), bf16[8,2,256,256]{3,2,1,0:T(8,128)(2,1)S(1)}, u32[]{:S(2)}, u32[]{:S(2)}) async-start(bf16[8,2,256,256]{3,2,1,0:T(8,128)(2,1)} %bitcast.54), calls=%async_computation.1 | async-start | bytes 4194304 | tf_op jit(solution)/shard_map/all_to_all | solution.py:44
  146.9 48.8 %all-to-all-done.1 = bf16[8,2,256,256]{3,2,1,0:T(8,128)(2,1)S(1)} async-done(((bf16[8,2,256,256]{3,2,1,0:T(8,128)(2,1)}), bf16[8,2,256,256]{3,2,1,0:T(8,128)(2,1)S(1)}, u32[]{:S(2)}, u32[]{:S(2)}) %all-to-all-start.1) | async-done | bytes 2097184 | tf_op jit(solution)/shard_map/all_to_all | solution.py:44
  195.7 1.3 copy-done.1
  197.0 2.8 %copy.21 = bf16[1,2,256,8,256]{2,4,3,1,0:T(8,128)(2,1)S(1)} copy(bf16[1,2,256,8,256]{4,2,1,3,0:T(8,128)(2,1)} %bitcast.53) | data formatting | bytes 4194304 | tf_op jit(solution)/shard_map/all_to_all | solution.py:44
  199.9 1.8 fusion.34
  201.7 1.6 copy.23
  203.2 0.3 fusion.27
  203.6 9.9 %reduce-window.6 = f32[2,4,16,128]{3,2,1,0:T(8,128)S(1)} reduce-window(f32[2,4,16,128]{3,2,1,0:T(8,128)S(1)} %copy.26, f32[]{:T(128)} %constant.9.clone.1), window={size=1x1x1x128 pad=0_0x0_0x0_0x0_127}, to_apply=%region_2.3 | reduce-window | flops 2080768 | bytes 131076 | tf_op jit(solution)/shard_map/reduce-window
  213.7 0.4 reduce-window.9
  214.3 1.4 copy.22
  215.7 1.7 fusion.16
  217.5 0.6 reshape.50
  218.1 1.4 copy.29
  219.5 1.4 copy.30
  (35 shorter events, 1.7 us)
Async XLA Ops:
  7.2 139.5 %copy-start = (f32[2,16]{1,0:T(2,128)S(1)}, f32[2,16]{1,0:T(2,128)}, u32[]{:S(2)}) copy-start(f32[2,16]{1,0:T(2,128)} %param.13) | copy-start | bytes 388
  7.2 93.5 %all-gather.2.cloned.1.call-start = ((), (), s32[]{:S(2)}) async-start(), calls=%async_computation.2 | async-start | bytes 10485760 | tf_op jit(solution)/shard_map/all_gather | solution.py:23
  10.3 0.7 copy-start.7
  10.3 1.6 copy-start.5
  10.3 90.4 %copy-start.8 = (f32[2048]{0:T(1024)S(1)}, f32[2048]{0:T(1024)}, u32[]{:S(2)}) copy-start(f32[2048]{0:T(1024)} %param.8) | copy-start | bytes 24580
  107.9 1.9 copy-start.2
  141.9 4.9 %copy-start.6 = (bf16[1,2,256]{2,1,0:T(2,128)(2,1)S(1)}, bf16[1,2,256]{2,1,0:T(2,128)(2,1)}, u32[]{:S(2)}) copy-start(bf16[1,2,256]{2,1,0:T(2,128)(2,1)} %param.12) | copy-start | bytes 3076
  141.9 53.8 %all-to-all-start.1 = ((bf16[8,2,256,256]{3,2,1,0:T(8,128)(2,1)}), bf16[8,2,256,256]{3,2,1,0:T(8,128)(2,1)S(1)}, u32[]{:S(2)}, u32[]{:S(2)}) async-start(bf16[8,2,256,256]{3,2,1,0:T(8,128)(2,1)} %bitcast.54), calls=%async_computation.1 | async-start | bytes 4194304 | tf_op jit(solution)/shard_map/all_to_all | solution.py:44
  195.7 1.3 copy-start.1
  201.7 12.6 %copy-start.4 = (bf16[1,1,256,2048]{2,3,1,0:T(8,128)(2,1)S(1)}, bf16[1,1,256,2048]{2,3,1,0:T(8,128)(2,1)}, u32[]{:S(2)}) copy-start(bf16[1,1,256,2048]{2,3,1,0:T(8,128)(2,1)} %get-tuple-element.9) | copy-start | bytes 3145732
  214.3 3.8 %copy-start.3 = (bf16[1,256,2048]{1,2,0:T(8,128)(2,1)S(1)}, bf16[1,256,2048]{1,2,0:T(8,128)(2,1)}, u32[]{:S(2)}) copy-start(bf16[1,256,2048]{1,2,0:T(8,128)(2,1)} %get-tuple-element.7) | copy-start | bytes 3145732
Sparse Core Ops, SparseCore 0:
  10.5 90.1 all-gather.1
